TPU v7x, 32 devices: a whole 2x2x4 slice. The times are simulated.
32 devices in a mesh: sp: 8 (over z, y), tp: 4 (over x, core).
Axes of the slice: x: 2, y: 2, z: 4, core: 2. Of those that a mesh axis runs over, the one named last changes fastest.
Arguments:
- queries: bfloat16 [2048, 2048], P('sp', 'tp'), may hold values from -16 to 16
- key_value_pairs: bfloat16 [2048, 512], P('sp', 'tp'), may hold values from -16 to 16
- forget_gate_total: float32 [2048, 32], P('sp', 'tp'), may hold values from -2048 to 0, as said below
- residual_in: bfloat16 [2048, 2048], P(('sp', 'tp')), may hold values from -12 to 12
- out_weight: bfloat16 [2048, 2048], P('tp'), may hold values from -0.25 to 0.25
- norm_gain: float32 [2048], replicated, may hold values from 0.1 to 1.9
- routes: int32 [2048, 2], P(('sp', 'tp')), may hold values from 0 to 7, all different within a row; in each aligned block of 64 rows (0 to 63, 64 to 127, ...) at most 24 rows name the same one
- route_weight: float32 [2048, 2], P(('sp', 'tp')), may hold values from 0.2 to 1
- expert_gate: bfloat16 [8, 2048, 3072], P('sp', None, 'tp'), may hold values from -0.125 to 0.125
- expert_up: bfloat16 [8, 2048, 3072], P('sp', None, 'tp'), may hold values from -0.125 to 0.125
- expert_down: bfloat16 [8, 3072, 2048], P('sp', 'tp'), may hold values from -0.109375 to 0.109375
Outputs:
- layer_out: bfloat16 [2048, 2048], P(('sp', 'tp'))
Inputs may be any that keep to these rules, and one draw needn't show every extreme that they name: `routes`: each row names 2 different experts; among the rows of one device no expert is named more than 24 times, and in every draw some device names some expert exactly 24 times. `forget_gate_total`: along the positions, each head's values never rise.
All inputs are finite; a program needn't handle non-finite values.
Results may differ from a plain program's by a relative error of at most 0.011.
Values may be sent and summed in bfloat16 or wider, within the bound.
A program may use at most 64 MiB of HBM per device.

v0:
```python
import math
import jax
import jax.numpy as jnp
from jax import lax
from jax.sharding import PartitionSpec as P

HEAD_SIZE = 64
NEG_FILL = -1e30
NORM_EPS = 1e-06


def slot_ranks(chosen, experts):
    onehot = (chosen[..., None] == jnp.arange(experts, dtype=jnp.int32)).astype(jnp.int32)
    earlier = jnp.cumsum(onehot, axis=-2) - onehot
    return jnp.sum(earlier * onehot, axis=-1)


def fill_slots(source_rows, target, slot_total, per_row):
    owner_slot = (
        jnp.zeros((slot_total,), jnp.int32)
        .at[target]
        .set(jnp.arange(1, target.shape[0] + 1, dtype=jnp.int32))
    )
    picked = source_rows[jnp.maximum(owner_slot - 1, 0) // per_row]
    return jnp.where((owner_slot > 0)[:, None], picked, jnp.zeros_like(picked))


def local(
    queries,
    key_value_pairs,
    forget_gate_total,
    residual_in,
    out_weight,
    norm_gain,
    routes,
    route_weight,
    expert_gate,
    expert_up,
    expert_down,
):
    seq_devices = lax.axis_size("sp")
    head_devices = lax.axis_size("tp")
    tok_rows = queries.shape[0]
    local_heads = queries.shape[1] // HEAD_SIZE
    local_groups = key_value_pairs.shape[1] // (2 * HEAD_SIZE)
    queries_per_group = local_heads // local_groups
    score_scale = HEAD_SIZE ** (-0.5)
    seq_index = lax.axis_index("sp")
    own_start = seq_index * tok_rows
    all_gates = lax.all_gather(forget_gate_total, "sp", axis=0, tiled=True)

    def attend_block(carried, query_set, kv_block, key_start):
        grouped_queries, query_gate, query_pos = query_set
        run_max, run_total, run_acc = carried
        key_count = kv_block.shape[0]
        key_value_head_list = kv_block.reshape(key_count, local_groups, 2 * HEAD_SIZE)
        scores = (
            jnp.einsum(
                "tkgd,skd->ktgs",
                grouped_queries,
                key_value_head_list[:, :, :HEAD_SIZE],
                preferred_element_type=jnp.float32,
            )
            * score_scale
        )
        gate_block = lax.dynamic_slice_in_dim(all_gates, key_start, key_count, 0)
        key_gate = gate_block.reshape(key_count, local_groups, queries_per_group).transpose(1, 2, 0)
        scores = scores + query_gate[..., None] - key_gate[:, None, :, :]
        key_pos = key_start + jnp.arange(key_count, dtype=jnp.int32)
        scores = jnp.where(
            key_pos[None, None, None, :] <= query_pos[None, :, None, None], scores, NEG_FILL
        )
        new_max = jnp.maximum(run_max, jnp.max(scores, axis=3))
        weights = jnp.exp(scores - new_max[..., None])
        rescale = jnp.exp(run_max - new_max)
        run_total = run_total * rescale + jnp.sum(weights, axis=3)
        block_sum = jnp.einsum(
            "ktgs,skd->ktgd",
            weights.astype(jnp.bfloat16),
            key_value_head_list[:, :, HEAD_SIZE:],
            preferred_element_type=jnp.float32,
        )
        return (new_max, run_total, run_acc * rescale[..., None] + block_sum)

    def start_state(row_count):
        return (
            jnp.full((local_groups, row_count, queries_per_group), NEG_FILL, jnp.float32),
            jnp.zeros((local_groups, row_count, queries_per_group), jnp.float32),
            jnp.zeros((local_groups, row_count, queries_per_group, HEAD_SIZE), jnp.float32),
        )

    row_count = queries.shape[0]
    grouped_queries = queries.reshape(row_count, local_groups, queries_per_group, HEAD_SIZE)
    query_gate = lax.dynamic_slice_in_dim(all_gates, own_start, row_count, 0)
    query_gate = query_gate.reshape(row_count, local_groups, queries_per_group).transpose(1, 0, 2)
    query_pos = own_start + jnp.arange(row_count, dtype=jnp.int32)
    query_sets = ((grouped_queries, query_gate, query_pos),)
    initial = tuple((start_state(query_set[2].shape[0]) for query_set in query_sets))
    kv_piece = lax.all_gather(key_value_pairs, "sp", axis=0, tiled=True)
    length = kv_piece.shape[0]
    key_block = math.gcd(length, 512)
    kv_blocks = kv_piece.reshape(length // key_block, key_block, kv_piece.shape[1])

    def one_block(block_index, inner_states):
        key_start = block_index * key_block
        updated = []
        for query_set, running in zip(query_sets, inner_states):
            last_pos = query_set[2][-1]
            updated.append(
                lax.cond(
                    key_start <= last_pos,
                    lambda state, chosen_set=query_set: attend_block(
                        state, chosen_set, kv_blocks[block_index], key_start
                    ),
                    lambda state: state,
                    running,
                )
            )
        return tuple(updated)

    states = lax.fori_loop(0, length // key_block, one_block, initial)
    run_max, run_total, run_acc = states[0]
    row_count = run_total.shape[1]
    attended = (
        (run_acc / run_total[..., None])
        .transpose(1, 0, 2, 3)
        .reshape(row_count, local_heads * HEAD_SIZE)
        .astype(jnp.bfloat16)
    )
    own_rows = tok_rows // head_devices
    row_block = attended
    mixed_rows = lax.psum_scatter(
        jnp.dot(row_block, out_weight, preferred_element_type=jnp.float32).astype(jnp.bfloat16),
        "tp",
        scatter_dimension=0,
        tiled=True,
    ).astype(jnp.float32)
    hidden_state = residual_in.astype(jnp.float32) + mixed_rows
    normed = (
        hidden_state
        * lax.rsqrt(jnp.mean(hidden_state * hidden_state, axis=1, keepdims=True) + NORM_EPS)
        * norm_gain
    ).astype(jnp.bfloat16)
    top_count = routes.shape[1]
    capacity = max(2, 3 * own_rows * top_count // (2 * seq_devices))
    model_width = normed.shape[1]
    chosen = routes.reshape(-1)
    target = chosen * capacity + slot_ranks(chosen, seq_devices)
    outgoing = fill_slots(normed, target, seq_devices * capacity, top_count).reshape(
        seq_devices, capacity, model_width
    )
    incoming = lax.all_to_all(outgoing, "sp", split_axis=0, concat_axis=0, tiled=True)
    arrived = lax.all_gather(incoming, "tp", axis=0, tiled=True)
    flat_in = arrived.reshape(-1, model_width)
    gate_value = jnp.dot(flat_in, expert_gate[0], preferred_element_type=jnp.float32)
    up_value = jnp.dot(flat_in, expert_up[0], preferred_element_type=jnp.float32)
    hidden_rows = (
        (jax.nn.silu(gate_value) * up_value)
        .astype(jnp.bfloat16)
        .reshape(arrived.shape[0], capacity, -1)
    )
    row_block = hidden_rows
    summed = lax.psum_scatter(
        jnp.einsum(
            "rcf,fd->rcd", row_block, expert_down[0], preferred_element_type=jnp.float32
        ).astype(jnp.bfloat16),
        "tp",
        scatter_dimension=0,
        tiled=True,
    )
    returned = lax.all_to_all(summed, "sp", split_axis=0, concat_axis=0, tiled=True)
    picked = returned.reshape(-1, model_width)[target].reshape(own_rows, top_count, model_width)
    combined = jnp.sum(picked.astype(jnp.float32) * route_weight[..., None], axis=1)
    return (hidden_state + combined).astype(jnp.bfloat16)


def solution(mesh):
    return jax.shard_map(
        local,
        mesh=mesh,
        in_specs=(
            P("sp", "tp"),
            P("sp", "tp"),
            P("sp", "tp"),
            P(("sp", "tp"), None),
            P("tp", None),
            P(),
            P(("sp", "tp"), None),
            P(("sp", "tp"), None),
            P("sp", None, "tp"),
            P("sp", None, "tp"),
            P("sp", "tp", None),
        ),
        out_specs=P(("sp", "tp"), None),
        check_vma=False,
    )
```

profile of v0, /device:TPU:0, one launch (start us, length us, event | category | flops | bytes accessed | tf_op | source)
XLA Modules:
  0.0 288.9 jit_solution(7621068759620404694)
XLA Ops:
  6.5 32.7 %all_gather.10 = f32[2048,8]{0,1:T(8,128)S(1)} all-gather(f32[256,8]{0,1:T(8,128)} %param.17), channel_id=1, replica_groups=mesh['sp'=8,'tp'=4] {'sp'}, dimensions={0}, use_global_device_ids=true | all-gather | bytes 73728 | tf_op jit(solution)/shard_map/all_gather | solution.py:50
  39.2 33.6 %all_gather.9 = bf16[2048,128]{1,0:T(8,128)(2,1)} all-gather(bf16[256,128]{1,0:T(8,128)(2,1)} %param.16), channel_id=1, replica_groups=mesh['sp'=8,'tp'=4] {'sp'}, dimensions={0}, use_global_device_ids=true | all-gather | bytes 589824 | tf_op jit(solution)/shard_map/all_gather | solution.py:99
  72.8 2.0 copy.25
  74.8 1.8 copy.24
  76.6 0.8 broadcast_in_dim.52
  77.4 10.9 %while.17 = (s32[]{:T(128)}, f32[1,256,8]{1,2,0:T(8,128)S(1)}, f32[1,256,8]{1,2,0:T(8,128)S(1)}, f32[1,256,8,64]{1,3,2,0:T(8,128)}, s32[256]{0:T(256)S(1)}, /*in...) while((s32[]{:T(128)}, f32[1,256,8]{1,2,0:T(8,128)S(1)}, ...), condition=%wide.region_5.6_spmd, body=%wide.region_0.5_spmd.sunk | while | flops 286661120 | bytes 19248544 | solution.py:121
  77.4 0.6 slice.26
  78.6 6.3 %conditional.2 = ((f32[1,256,8]{1,2,0:T(8,128)S(1)}, f32[1,256,8]{1,2,0:T(8,128)S(1)}, f32[1,256,8,64]{1,3,2,0:T(8,128)})) conditional(s32[]{:T(128)} %convert_element_type.90, (f32[1,256,8]{1,2,0:T(8,128)S(1)}, f32[1,256,8]{1,2,0:T(8,128)S(1)}, f32[1,256,8,64]{1,3,2,0:T(8,128)}) %tuple.41, (s32[]{:T(128)}, s32[256]{0:T(256)S(1)}, s32[]{:T(128)}, ...), branch_computations={%region_1.0_spmd, %region_2.4_spmd} | conditional | flops 286661120 | bytes 19248296 | solution.py:110
  78.6 0.9 dynamic-slice_bitcast_fusion
  79.6 0.1 broadcast_compare_fusion
  79.7 2.1 fusion.3
  81.9 1.5 fusion.10
  83.4 1.4 fusion.2
  84.9 0.6 slice.26
  86.0 0.6 slice.26
  87.2 0.6 slice.26
  88.4 1.1 divide_convert_fusion
  89.5 3.3 %convolution_convert_fusion.1 = bf16[256,2048]{1,0:T(8,128)(2,1)} fusion(bf16[256,512]{0,1:T(8,128)(2,1)S(1)} %bitcast.88, bf16[512,2048]{1,0:T(8,128)(2,1)} %param.19), kind=kOutput, calls=%fused_computation.33 | convolution fusion | flops 537395200 | bytes 3407872 | tf_op jit(solution)/shard_map/dot_general | solution.py:133
  92.9 0.0 all-gather.2.cloned.1.call-start
  92.9 0.1 copy.27
  93.0 0.1 eq.15
  93.2 0.1 fusion.25
  93.3 0.2 reduce_window_sum.11
  93.4 0.1 copy.26
  93.5 0.1 mul.84
  93.7 0.2 select_reduce_fusion
  93.9 1.0 scatter_custom_fusion
  94.9 0.1 broadcast_in_dim.53
  95.0 42.6 %reduce-scatter.3.cloned.1.call-done = bf16[64,2048]{1,0:T(8,128)(2,1)} async-done(((bf16[256,2048]{1,0:T(8,128)(2,1)}), bf16[64,2048]{1,0:T(8,128)(2,1)}) %reduce-scatter.3.cloned.1.call-update) | async-done | bytes 262160 | tf_op jit(solution)/shard_map/reduce_scatter | solution.py:132
  137.6 1.1 multiply_reduce_fusion.1
  138.8 1.1 multiply_convert_fusion.1
  139.9 2.0 gather_fusion
  141.9 1.3 broadcast_select_fusion
  143.2 25.4 %all_to_all.10 = bf16[8,24,2048]{2,1,0:T(8,128)(2,1)} all-to-all(bf16[8,24,2048]{2,1,0:T(8,128)(2,1)S(1)} %broadcast_select_fusion), channel_id=1, replica_groups=mesh['sp'=8,'tp'=4] {'sp'}, dimensions={0} | all-to-all | bytes 1572864 | tf_op jit(solution)/shard_map/all_to_all | solution.py:152
  168.6 0.0 all-gather.2.cloned.1.call-update
  168.6 0.2 reduce-scatter.5.cloned.1.call-start
  168.9 26.5 %all-gather.2.cloned.1.call-done = bf16[32,24,2048]{2,1,0:T(8,128)(2,1)} async-done(((bf16[8,24,2048]{2,1,0:T(8,128)(2,1)}), bf16[32,24,2048]{2,1,0:T(8,128)(2,1)}) %all-gather.2.cloned.1.call-update) | async-done | bytes 3145744 | tf_op jit(solution)/shard_map/all_gather | solution.py:153
  195.4 5.6 %fusion.19 = f32[768,768]{1,0:T(8,128)S(1)} fusion(bf16[768,2048]{1,0:T(8,128)(2,1)} %bitcast.91, bf16[1,2048,768]{2,1,0:T(8,128)(2,1)} %param.24), kind=kOutput, calls=%fused_computation.29 | convolution fusion | flops 2415919104 | bytes 8650752 | tf_op jit(solution)/shard_map/dot_general | solution.py:156
  201.0 2.9 multiply_convert_fusion
  203.9 4.0 %convolution_convert_fusion = bf16[32,24,2048]{2,1,0:T(8,128)(2,1)} fusion(bf16[32,24,768]{2,1,0:T(8,128)(2,1)S(1)} %bitcast.93, bf16[1,768,2048]{2,1,0:T(8,128)(2,1)S(1)} %copy-done), kind=kOutput, calls=%fused_computation.27 | convolution fusion | flops 2417491968 | bytes 7471104 | tf_op jit(solution)/shard_map/rcf,fd->rcd/dot_general | solution.py:164
  207.9 38.0 %reduce-scatter.5.cloned.1.call-done = bf16[8,24,2048]{2,1,0:T(8,128)(2,1)} async-done(((bf16[32,24,2048]{2,1,0:T(8,128)(2,1)}), bf16[8,24,2048]{2,1,0:T(8,128)(2,1)}) %reduce-scatter.5.cloned.1.call-update) | async-done | bytes 786448 | tf_op jit(solution)/shard_map/reduce_scatter | solution.py:163
  245.9 5.5 %all-to-all-start.1 = ((bf16[8,24,2048]{2,1,0:T(8,128)(2,1)}), bf16[8,24,2048]{2,1,0:T(8,128)(2,1)}, u32[]{:S(2)}, u32[]{:S(2)}) async-start(bf16[8,24,2048]{2,1,0:T(8,128)(2,1)} %reduce-scatter.5.cloned.1.call-done), calls=%async_computation.3 | async-start | bytes 1572864 | tf_op jit(solution)/shard_map/all_to_all | solution.py:171
  251.5 0.1 copy.28
  251.6 20.1 %all-to-all-done.1 = bf16[8,24,2048]{2,1,0:T(8,128)(2,1)} async-done(((bf16[8,24,2048]{2,1,0:T(8,128)(2,1)}), bf16[8,24,2048]{2,1,0:T(8,128)(2,1)}, u32[]{:S(2)}, u32[]{:S(2)}) %all-to-all-start.1) | async-done | bytes 786464 | tf_op jit(solution)/shard_map/all_to_all | solution.py:171
  271.6 3.5 %gather_fusion.1 = bf16[128,2048]{1,0:T(8,128)(2,1)} fusion(bf16[192,2048]{1,0:T(8,128)(2,1)} %bitcast.29, s32[1024]{0:T(1024)S(1)} %pad_clamp_fusion), kind=kCustom, calls=%fused_computation.1 | custom fusion | bytes 1049088 | tf_op jit(solution)/shard_map/gather | solution.py:172
  275.2 2.7 reshape.150
  277.8 2.8 multiply_reduce_fusion
  280.7 1.8 add_convert_fusion
  (43 shorter events, 0.2 us)
Async XLA Ops:
  6.5 197.3 %copy-start = (bf16[1,768,2048]{2,1,0:T(8,128)(2,1)S(1)}, bf16[1,768,2048]{2,1,0:T(8,128)(2,1)}, u32[]{:S(2)}) copy-start(bf16[1,768,2048]{2,1,0:T(8,128)(2,1)} %param.25) | copy-start | bytes 9437188
  6.5 131.1 %reduce-scatter.3.cloned.1.call-start = ((), (), s32[]{:S(2)}) async-start(), calls=%async_computation.4 | async-start | bytes 1310720 | tf_op jit(solution)/shard_map/reduce_scatter | solution.py:132
  79.7 2.2 copy-start.3
  83.4 1.4 copy-start.4
  88.4 4.5 %copy-start.6 = (s32[64,2]{0,1:T(2,128)S(1)}, s32[64,2]{0,1:T(2,128)}, u32[]{:S(2)}) copy-start(s32[64,2]{0,1:T(2,128)} %param.21) | copy-start | bytes 1540
  88.4 49.2 %copy-start.1 = (bf16[64,2048]{1,0:T(8,128)(2,1)S(1)}, bf16[64,2048]{1,0:T(8,128)(2,1)}, u32[]{:S(2)}) copy-start(bf16[64,2048]{1,0:T(8,128)(2,1)} %param.18) | copy-start | bytes 786436
  88.4 50.4 %copy-start.5 = (f32[2048]{0:T(1024)S(1)}, f32[2048]{0:T(1024)}, u32[]{:S(2)}) copy-start(f32[2048]{0:T(1024)} %param.20) | copy-start | bytes 24580
  92.9 102.5 %all-gather.2.cloned.1.call-start = ((), (), s32[]{:S(2)}) async-start(), calls=%async_computation.5 | async-start | bytes 3932160 | tf_op jit(solution)/shard_map/all_gather | solution.py:153
  168.6 77.3 %reduce-scatter.5.cloned.1.call-start = ((), (), s32[]{:S(2)}) async-start(), calls=%async_computation.6 | async-start | bytes 3932160 | tf_op jit(solution)/shard_map/reduce_scatter | solution.py:163
  195.4 5.6 %copy-start.8 = (bf16[1,2048,768]{2,1,0:T(8,128)(2,1)S(1)}, bf16[1,2048,768]{2,1,0:T(8,128)(2,1)}, u32[]{:S(2)}) copy-start(bf16[1,2048,768]{2,1,0:T(8,128)(2,1)} %param.23) | copy-start | bytes 9437188
  195.4 5.6 %copy-start.9 = (bf16[32,24,2048]{2,1,0:T(8,128)(2,1)S(1)}, bf16[32,24,2048]{2,1,0:T(8,128)(2,1)}, u32[]{:S(2)}) copy-start(bf16[32,24,2048]{2,1,0:T(8,128)(2,1)} %all-gather.2.cloned.1.call-done) | copy-start | bytes 9437188
  207.9 43.6 %copy-start.7 = (f32[64,2]{0,1:T(2,128)S(1)}, f32[64,2]{0,1:T(2,128)}, u32[]{:S(2)}) copy-start(f32[64,2]{0,1:T(2,128)} %param.22) | copy-start | bytes 1540
  245.9 25.7 %all-to-all-start.1 = ((bf16[8,24,2048]{2,1,0:T(8,128)(2,1)}), bf16[8,24,2048]{2,1,0:T(8,128)(2,1)}, u32[]{:S(2)}, u32[]{:S(2)}) async-start(bf16[8,24,2048]{2,1,0:T(8,128)(2,1)} %reduce-scatter.5.cloned.1.call-done), calls=%async_computation.3 | async-start | bytes 1572864 | tf_op jit(solution)/shard_map/all_to_all | solution.py:171
  271.6 9.0 %copy-start.2 = (bf16[64,2048]{1,0:T(8,128)(2,1)S(1)}, bf16[64,2048]{1,0:T(8,128)(2,1)}, u32[]{:S(2)}) copy-start(bf16[64,2048]{1,0:T(8,128)(2,1)} %param.18) | copy-start | bytes 786436
Sparse Core Ops, SparseCore 0:
  93.0 44.5 reduce-scatter.2
  168.8 26.5 all-gather.1
  208.0 37.8 reduce-scatter.4
where the time goes:
time: 290 us; the launch traced here: 289 us
  waiting for transfers between devices  127 us (44%)
  blocking collectives  91.7 us (32%)
  matrix products  19.4 us (7%)
  local copies, waits for them, and re-layouts  17.7 us (6%)
  between operations  13.3 us (5%)
  other arithmetic  11.2 us (4%)
  starting transfers between devices  5.78 us (2%)
    reduce_scatter x1, waiting for transfers between devices, local(): lax.psum_scatter(jnp.dot(row_block, out_weight, preferred_element_type=jn...  42.6 us
    reduce_scatter x1, waiting for transfers between devices, local(): lax.psum_scatter(jnp.einsum('rcf,fd->rcd', row_block, expert_down[0], pre...  38 us
    all_gather x1, blocking collectives, local(): kv_piece = lax.all_gather(key_value_pairs, 'sp', axis=0, tiled=True)  33.6 us
    all_gather x1, blocking collectives, local(): all_gates = lax.all_gather(forget_gate_total, 'sp', axis=0, tiled=True)  32.7 us
    all_gather x1, waiting for transfers between devices, local(): arrived = lax.all_gather(incoming, 'tp', axis=0, tiled=True)  26.5 us
    all_to_all x1, blocking collectives, local(): lax.all_to_all(outgoing, 'sp', split_axis=0, concat_axis=0, tiled=True)  25.4 us
    all_to_all x1, waiting for transfers between devices, local(): lax.all_to_all(summed, 'sp', split_axis=0, concat_axis=0, tiled=True)  20.1 us
  transfers between devices with their start and end apart: 4, of which 4 were waited for; matrix products, arithmetic and copies ran while one was open for 1% of the time, Pallas kernels for 0%

commit v1 on v0

--- a/solution.py
+++ b/solution.py
@@ -47,7 +47,9 @@
     score_scale = HEAD_SIZE ** (-0.5)
     seq_index = lax.axis_index("sp")
     own_start = seq_index * tok_rows
-    all_gates = lax.all_gather(forget_gate_total, "sp", axis=0, tiled=True)
+    all_gates = jnp.concatenate(
+        lax.all_to_all(jnp.stack([forget_gate_total] * lax.axis_size("sp")), "sp", 0, 0), axis=0
+    )
 
     def attend_block(carried, query_set, kv_block, key_start):
         grouped_queries, query_gate, query_pos = query_set

time: 290 us -> 267 us (0.921)
  blocking collectives: 91.7 us -> 59.4 us
  starting transfers between devices: 5.78 us -> 13.1 us
    all_gather x1 -> x0, blocking collectives: 32.7 us -> none  [local(): all_gates = lax.all_gather(forget_gate_total, 'sp', axis=0, tiled=True)]
    all_to_all x0 -> x1, starting transfers between devices: none -> 7.31 us  [local(): lax.all_to_all(jnp.stack([forget_gate_total] * lax.axis_size('sp')), 'sp'...]
  transfers between devices with their start and end apart: 4 -> 5, of which waited for: 4 -> 4; matrix products, arithmetic and copies ran while one was open for 1% -> 2% of each run, Pallas kernels for 0% -> 0%
where the time goes in v1:
time: 267 us; the launch traced here: 266 us
  waiting for transfers between devices  127 us (48%)
  blocking collectives  59.4 us (22%)
  local copies, waits for them, and re-layouts  19.6 us (7%)
  matrix products  19.4 us (7%)
  between operations  13.3 us (5%)
  starting transfers between devices  13.1 us (5%)
  other arithmetic  11.2 us (4%)
  loops' own time  3 us (1%)
    reduce_scatter x1, waiting for transfers between devices, local(): lax.psum_scatter(jnp.dot(row_block, out_weight, preferred_element_type=jn...  42.6 us
    reduce_scatter x1, waiting for transfers between devices, local(): lax.psum_scatter(jnp.einsum('rcf,fd->rcd', row_block, expert_down[0], pre...  38 us
    all_gather x1, blocking collectives, local(): kv_piece = lax.all_gather(key_value_pairs, 'sp', axis=0, tiled=True)  34 us
    all_gather x1, waiting for transfers between devices, local(): arrived = lax.all_gather(incoming, 'tp', axis=0, tiled=True)  26.5 us
    all_to_all x1, blocking collectives, local(): lax.all_to_all(outgoing, 'sp', split_axis=0, concat_axis=0, tiled=True)  25.4 us
    all_to_all x1, waiting for transfers between devices, local(): lax.all_to_all(summed, 'sp', split_axis=0, concat_axis=0, tiled=True)  20.1 us
    all_to_all x1, starting transfers between devices, local(): lax.all_to_all(jnp.stack([forget_gate_total] * lax.axis_size('sp')), 'sp'...  7.31 us
    dot_general x1, matrix products, local(): jnp.dot(flat_in, expert_up[0], preferred_element_type=jnp.float32)  5.58 us
  transfers between devices with their start and end apart: 5, of which 4 were waited for; matrix products, arithmetic and copies ran while one was open for 2% of the time, Pallas kernels for 0%

profile of v1, /device:TPU:0, one launch (start us, length us, event | category | flops | bytes accessed | tf_op | source)
XLA Modules:
  0.0 266.4 jit_solution(7033059360013481821)
XLA Ops:
  6.5 1.5 stack.2
  8.0 7.3 %all-to-all-start = ((f32[8,256,8]{1,2,0:T(8,128)}), f32[8,256,8]{1,2,0:T(8,128)S(1)}, u32[]{:S(2)}, u32[]{:S(2)}) async-start(f32[8,256,8]{1,2,0:T(8,128)} %stack.2), calls=%async_computation | async-start | bytes 131072 | tf_op jit(solution)/shard_map/all_to_all | solution.py:51
  15.4 34.0 %all_gather.6 = bf16[2048,128]{1,0:T(8,128)(2,1)} all-gather(bf16[256,128]{1,0:T(8,128)(2,1)} %param.16), channel_id=1, replica_groups=mesh['sp'=8,'tp'=4] {'sp'}, dimensions={0}, use_global_device_ids=true | all-gather | bytes 589824 | tf_op jit(solution)/shard_map/all_gather | solution.py:101
  49.4 2.0 copy.25
  51.4 1.8 copy.24
  53.2 0.8 broadcast_in_dim.52
  54.0 11.7 %while.17 = (s32[]{:T(128)}, f32[1,256,8]{1,2,0:T(8,128)S(1)}, f32[1,256,8]{1,2,0:T(8,128)S(1)}, f32[1,256,8,64]{1,3,2,0:T(8,128)}, s32[256]{0:T(256)S(1)}, /*in...) while((s32[]{:T(128)}, f32[1,256,8]{1,2,0:T(8,128)S(1)}, ...), condition=%wide.region_5.6_spmd, body=%wide.region_0.5_spmd.sunk | while | flops 286661120 | bytes 19248544 | solution.py:123
  54.0 0.6 slice.26
  55.4 6.3 %conditional.2 = ((f32[1,256,8]{1,2,0:T(8,128)S(1)}, f32[1,256,8]{1,2,0:T(8,128)S(1)}, f32[1,256,8,64]{1,3,2,0:T(8,128)})) conditional(s32[]{:T(128)} %convert_element_type.90, (f32[1,256,8]{1,2,0:T(8,128)S(1)}, f32[1,256,8]{1,2,0:T(8,128)S(1)}, f32[1,256,8,64]{1,3,2,0:T(8,128)}) %tuple.41, (s32[]{:T(128)}, s32[256]{0:T(256)S(1)}, s32[]{:T(128)}, ...), branch_computations={%region_1.0_spmd, %region_2.4_spmd} | conditional | flops 286661120 | bytes 19248296 | solution.py:112
  55.4 0.9 dynamic-slice_bitcast_fusion
  56.4 0.1 broadcast_compare_fusion
  56.5 2.1 fusion.3
  58.7 1.5 fusion.10
  60.2 1.4 fusion.2
  61.7 0.7 slice.26
  63.1 0.7 slice.26
  64.4 0.7 slice.26
  65.8 1.1 divide_convert_fusion
  67.0 3.3 %convolution_convert_fusion.1 = bf16[256,2048]{1,0:T(8,128)(2,1)} fusion(bf16[256,512]{0,1:T(8,128)(2,1)S(1)} %bitcast.89, bf16[512,2048]{1,0:T(8,128)(2,1)} %param.19), kind=kOutput, calls=%fused_computation.33 | convolution fusion | flops 537395200 | bytes 3407872 | tf_op jit(solution)/shard_map/dot_general | solution.py:135
  70.3 0.0 all-gather.2.cloned.1.call-start
  70.3 0.1 copy.27
  70.4 0.1 eq.15
  70.6 0.1 fusion.25
  70.7 0.2 reduce_window_sum.11
  70.8 0.1 copy.26
  70.9 0.1 mul.84
  71.1 0.2 select_reduce_fusion
  71.3 1.0 scatter_custom_fusion
  72.3 0.1 broadcast_in_dim.53
  72.4 42.6 %reduce-scatter.3.cloned.1.call-done = bf16[64,2048]{1,0:T(8,128)(2,1)} async-done(((bf16[256,2048]{1,0:T(8,128)(2,1)}), bf16[64,2048]{1,0:T(8,128)(2,1)}) %reduce-scatter.3.cloned.1.call-update) | async-done | bytes 262160 | tf_op jit(solution)/shard_map/reduce_scatter | solution.py:134
  115.0 1.1 multiply_reduce_fusion.1
  116.2 1.1 multiply_convert_fusion.1
  117.4 2.0 gather_fusion
  119.4 1.3 broadcast_select_fusion
  120.7 25.4 %all_to_all.15 = bf16[8,24,2048]{2,1,0:T(8,128)(2,1)} all-to-all(bf16[8,24,2048]{2,1,0:T(8,128)(2,1)S(1)} %broadcast_select_fusion), channel_id=1, replica_groups=mesh['sp'=8,'tp'=4] {'sp'}, dimensions={0} | all-to-all | bytes 1572864 | tf_op jit(solution)/shard_map/all_to_all | solution.py:154
  146.1 0.2 reduce-scatter.5.cloned.1.call-start
  146.3 26.5 %all-gather.2.cloned.1.call-done = bf16[32,24,2048]{2,1,0:T(8,128)(2,1)} async-done(((bf16[8,24,2048]{2,1,0:T(8,128)(2,1)}), bf16[32,24,2048]{2,1,0:T(8,128)(2,1)}) %all-gather.2.cloned.1.call-update) | async-done | bytes 3145744 | tf_op jit(solution)/shard_map/all_gather | solution.py:155
  172.8 5.6 %fusion.19 = f32[768,768]{1,0:T(8,128)S(1)} fusion(bf16[768,2048]{1,0:T(8,128)(2,1)} %bitcast.94, bf16[1,2048,768]{2,1,0:T(8,128)(2,1)} %param.24), kind=kOutput, calls=%fused_computation.29 | convolution fusion | flops 2415919104 | bytes 8650752 | tf_op jit(solution)/shard_map/dot_general | solution.py:158
  178.4 2.9 %multiply_convert_fusion = bf16[768,768]{1,0:T(8,128)(2,1)S(1)} fusion(f32[768,768]{1,0:T(8,128)S(1)} %fusion.19, bf16[768,2048]{1,0:T(8,128)(2,1)S(1)} %bitcast.95, bf16[1,2048,768]{2,1,0:T(8,128)(2,1)S(1)} %copy-done.8), kind=kOutput, calls=%fused_computation.34 | convolution fusion | flops 2419458048 | bytes 9830400 | tf_op jit(solution)/shard_map/dot_general | solution.py:157
  181.3 4.0 %convolution_convert_fusion = bf16[32,24,2048]{2,1,0:T(8,128)(2,1)} fusion(bf16[32,24,768]{2,1,0:T(8,128)(2,1)S(1)} %bitcast.96, bf16[1,768,2048]{2,1,0:T(8,128)(2,1)S(1)} %copy-done), kind=kOutput, calls=%fused_computation.27 | convolution fusion | flops 2417491968 | bytes 7471104 | tf_op jit(solution)/shard_map/rcf,fd->rcd/dot_general | solution.py:166
  185.3 38.0 %reduce-scatter.5.cloned.1.call-done = bf16[8,24,2048]{2,1,0:T(8,128)(2,1)} async-done(((bf16[32,24,2048]{2,1,0:T(8,128)(2,1)}), bf16[8,24,2048]{2,1,0:T(8,128)(2,1)}) %reduce-scatter.5.cloned.1.call-update) | async-done | bytes 786448 | tf_op jit(solution)/shard_map/reduce_scatter | solution.py:165
  223.4 5.5 %all-to-all-start.2 = ((bf16[8,24,2048]{2,1,0:T(8,128)(2,1)}), bf16[8,24,2048]{2,1,0:T(8,128)(2,1)}, u32[]{:S(2)}, u32[]{:S(2)}) async-start(bf16[8,24,2048]{2,1,0:T(8,128)(2,1)} %reduce-scatter.5.cloned.1.call-done), calls=%async_computation.4 | async-start | bytes 1572864 | tf_op jit(solution)/shard_map/all_to_all | solution.py:173
  228.9 0.1 copy.28
  229.0 20.1 %all-to-all-done.2 = bf16[8,24,2048]{2,1,0:T(8,128)(2,1)} async-done(((bf16[8,24,2048]{2,1,0:T(8,128)(2,1)}), bf16[8,24,2048]{2,1,0:T(8,128)(2,1)}, u32[]{:S(2)}, u32[]{:S(2)}) %all-to-all-start.2) | async-done | bytes 786464 | tf_op jit(solution)/shard_map/all_to_all | solution.py:173
  249.1 3.5 %gather_fusion.1 = bf16[128,2048]{1,0:T(8,128)(2,1)} fusion(bf16[192,2048]{1,0:T(8,128)(2,1)} %bitcast.30, s32[1024]{0:T(1024)S(1)} %pad_clamp_fusion), kind=kCustom, calls=%fused_computation.1 | custom fusion | bytes 1049088 | tf_op jit(solution)/shard_map/gather | solution.py:174
  252.6 2.7 reshape.156
  255.3 2.8 %multiply_reduce_fusion = f32[64,2048]{1,0:T(8,128)S(1)} fusion(f32[64,2,2048]{2,1,0:T(2,128)} %reshape.156, f32[64,2]{1,0:T(8,128)S(1)} %copy.28), kind=kLoop, calls=%fused_computation.35 | loop fusion | flops 393216 | bytes 1573376 | tf_op jit(solution)/shard_map/reduce_sum | solution.py:175
  258.1 1.8 add_convert_fusion
  (45 shorter events, 0.3 us)
Async XLA Ops:
  6.5 174.7 %copy-start = (bf16[1,768,2048]{2,1,0:T(8,128)(2,1)S(1)}, bf16[1,768,2048]{2,1,0:T(8,128)(2,1)}, u32[]{:S(2)}) copy-start(bf16[1,768,2048]{2,1,0:T(8,128)(2,1)} %param.25) | copy-start | bytes 9437188
  8.0 45.2 %all-to-all-start = ((f32[8,256,8]{1,2,0:T(8,128)}), f32[8,256,8]{1,2,0:T(8,128)S(1)}, u32[]{:S(2)}, u32[]{:S(2)}) async-start(f32[8,256,8]{1,2,0:T(8,128)} %stack.2), calls=%async_computation | async-start | bytes 131072 | tf_op jit(solution)/shard_map/all_to_all | solution.py:51
  15.3 99.7 %reduce-scatter.3.cloned.1.call-start = ((), (), s32[]{:S(2)}) async-start(), calls=%async_computation.5 | async-start | bytes 1310720 | tf_op jit(solution)/shard_map/reduce_scatter | solution.py:134
  56.5 2.2 copy-start.3
  60.2 1.4 copy-start.4
  65.8 4.5 %copy-start.6 = (s32[64,2]{0,1:T(2,128)S(1)}, s32[64,2]{0,1:T(2,128)}, u32[]{:S(2)}) copy-start(s32[64,2]{0,1:T(2,128)} %param.21) | copy-start | bytes 1540
  65.8 49.2 %copy-start.1 = (bf16[64,2048]{1,0:T(8,128)(2,1)S(1)}, bf16[64,2048]{1,0:T(8,128)(2,1)}, u32[]{:S(2)}) copy-start(bf16[64,2048]{1,0:T(8,128)(2,1)} %param.18) | copy-start | bytes 786436
  65.8 50.4 %copy-start.5 = (f32[2048]{0:T(1024)S(1)}, f32[2048]{0:T(1024)}, u32[]{:S(2)}) copy-start(f32[2048]{0:T(1024)} %param.20) | copy-start | bytes 24580
  70.3 102.5 %all-gather.2.cloned.1.call-start = ((), (), s32[]{:S(2)}) async-start(), calls=%async_computation.6 | async-start | bytes 3932160 | tf_op jit(solution)/shard_map/all_gather | solution.py:155
  146.1 77.3 %reduce-scatter.5.cloned.1.call-start = ((), (), s32[]{:S(2)}) async-start(), calls=%async_computation.7 | async-start | bytes 3932160 | tf_op jit(solution)/shard_map/reduce_scatter | solution.py:165
  172.8 5.6 %copy-start.8 = (bf16[1,2048,768]{2,1,0:T(8,128)(2,1)S(1)}, bf16[1,2048,768]{2,1,0:T(8,128)(2,1)}, u32[]{:S(2)}) copy-start(bf16[1,2048,768]{2,1,0:T(8,128)(2,1)} %param.23) | copy-start | bytes 9437188
  172.8 5.6 %copy-start.9 = (bf16[32,24,2048]{2,1,0:T(8,128)(2,1)S(1)}, bf16[32,24,2048]{2,1,0:T(8,128)(2,1)}, u32[]{:S(2)}) copy-start(bf16[32,24,2048]{2,1,0:T(8,128)(2,1)} %all-gather.2.cloned.1.call-done) | copy-start | bytes 9437188
  185.3 43.6 %copy-start.7 = (f32[64,2]{0,1:T(2,128)S(1)}, f32[64,2]{0,1:T(2,128)}, u32[]{:S(2)}) copy-start(f32[64,2]{0,1:T(2,128)} %param.22) | copy-start | bytes 1540
  223.4 25.7 %all-to-all-start.2 = ((bf16[8,24,2048]{2,1,0:T(8,128)(2,1)}), bf16[8,24,2048]{2,1,0:T(8,128)(2,1)}, u32[]{:S(2)}, u32[]{:S(2)}) async-start(bf16[8,24,2048]{2,1,0:T(8,128)(2,1)} %reduce-scatter.5.cloned.1.call-done), calls=%async_computation.4 | async-start | bytes 1572864 | tf_op jit(solution)/shard_map/all_to_all | solution.py:173
  249.1 9.0 %copy-start.2 = (bf16[64,2048]{1,0:T(8,128)(2,1)S(1)}, bf16[64,2048]{1,0:T(8,128)(2,1)}, u32[]{:S(2)}) copy-start(bf16[64,2048]{1,0:T(8,128)(2,1)} %param.18) | copy-start | bytes 786436
Sparse Core Ops, SparseCore 0:
  70.4 44.6 reduce-scatter.2
  146.2 26.5 all-gather.1
  185.5 37.8 reduce-scatter.4
